TPU v7x, 32 devices: a whole 2x2x4 slice. The times are simulated.
32 devices in a mesh: sp: 8 (over z, y), tp: 4 (over x, core).
Axes of the slice: x: 2, y: 2, z: 4, core: 2. Of those that a mesh axis runs over, the one named last changes fastest.
Arguments:
- queries: bfloat16 [8192, 8, 128], P('sp', 'tp'), may hold values from -160 to 160
- keys_values: bfloat16 [8192, 8, 128], P('sp', 'tp'), may hold values from -5 to 5
- sink_logits: float32 [8, 2], P('tp'), may hold values from 2 to 7
- doc_ids: int32 [8192], replicated, may hold values from 0 to 5, never falling along the last dimension, each value on 1 to 4096 neighbouring positions
- residual: bfloat16 [8192, 2048], P('sp'), may hold values from -6 to 6
- out_weight: bfloat16 [1024, 2048], P('tp'), may hold values from -1.5 to 1.5
- ffn_gain: float32 [2048], replicated, may hold values from 0.1 to 1.9
- gate_weight: bfloat16 [2048, 5120], P('sp', 'tp'), may hold values from -0.125 to 0.125
- value_weight: bfloat16 [2048, 5120], P('sp', 'tp'), may hold values from -0.125 to 0.125
- conv_taps: float32 [3, 5120], P(None, 'tp'), may hold values from -4 to 4
- down_weight: bfloat16 [2048, 5120], P('sp', 'tp'), may hold values from -0.078125 to 0.078125
Outputs:
- layer_out: bfloat16 [8192, 2048], P(('sp', 'tp'))
Inputs may be any that keep to these rules, and one draw needn't show every extreme that they name: `doc_ids`: document numbers never fall along the sequence; a document spans at most 4096 positions.
All inputs are finite; a program needn't handle non-finite values.
Results may differ from a plain program's by a relative error of at most 0.02.
Values may be sent and summed in bfloat16 or wider, within the bound.
A program may use at most 128 MiB of HBM per device.

v0:
```python
import jax
import jax.numpy as jnp
from jax import lax
from jax.sharding import PartitionSpec as P

HEAD_DIM = 64
WINDOW = 128
norm_epsilon = 1e-06
masked_score = -1e30
contract_last = (((1,), (1,)), ((), ()))


def extended_2(cells, sides, width):
    for axis, dim in sides:
        count = lax.axis_size(axis)
        ends = count - 1
        head = lax.slice_in_dim(cells, 0, width, axis=dim)
        tail = lax.slice_in_dim(cells, cells.shape[dim] - width, cells.shape[dim], axis=dim)
        cells = jnp.concatenate(
            [
                lax.ppermute(tail, axis, [(i, (i + 1) % count) for i in range(ends)]),
                cells,
                lax.ppermute(head, axis, [((i + 1) % count, i) for i in range(ends)]),
            ],
            axis=dim,
        )
    return cells


def band_blocks(padded, block_count, window_rows):
    row_block = padded.reshape((block_count + 2, window_rows) + padded.shape[1:])
    return jnp.concatenate([row_block[:-2], row_block[1:-1], row_block[2:]], axis=1)


def normalize(stream, gain):
    stream_f = stream.astype(jnp.float32)
    scale = lax.rsqrt(jnp.mean(stream_f * stream_f, axis=-1, keepdims=True) + norm_epsilon)
    return (stream_f * scale * gain).astype(jnp.bfloat16)


def attend(queries, keys_values, sink_logits, doc_ids, offset):
    local_rows = queries.shape[0]
    kv_local = queries.shape[1]
    head_dim = HEAD_DIM
    group_size = queries.shape[2] // head_dim
    window_rows = WINDOW
    block_count = local_rows // window_rows
    padded = extended_2(keys_values, (("sp", 0),), window_rows)
    blocks = band_blocks(padded, block_count, window_rows)
    key_blocks = blocks[..., :head_dim]
    value_blocks = blocks[..., head_dim:]
    query_blocks = queries.reshape(block_count, window_rows, kv_local, group_size, head_dim)
    scores = jnp.einsum(
        "nqkgd,nskd->nkgqs", query_blocks, key_blocks, preferred_element_type=jnp.float32
    ) * head_dim ** (-0.5)
    padded_docs = jnp.pad(doc_ids, window_rows, constant_values=-1)
    near_docs = lax.dynamic_slice_in_dim(padded_docs, offset, local_rows + 2 * window_rows)
    key_docs = band_blocks(near_docs, block_count, window_rows)
    query_docs = near_docs[window_rows : window_rows + local_rows].reshape(block_count, window_rows)
    distance = jnp.arange(window_rows)[:, None] + window_rows - jnp.arange(3 * window_rows)[None, :]
    allowed = (jnp.abs(distance) <= WINDOW)[None] & (query_docs[:, :, None] == key_docs[:, None, :])
    scores = jnp.where(allowed[:, None, None], scores, masked_score)
    sink_part = sink_logits[None, :, :, None, None]
    top_score = jnp.maximum(jnp.max(scores, axis=-1, keepdims=True), sink_part)
    exp_scores = jnp.exp(scores - top_score)
    denominator = jnp.sum(exp_scores, axis=-1, keepdims=True) + jnp.exp(sink_part - top_score)
    probs = (exp_scores / denominator).astype(jnp.bfloat16)
    result = jnp.einsum(
        "nkgqs,nskd->nqkgd", probs, value_blocks, preferred_element_type=jnp.float32
    )
    return result.reshape(local_rows, kv_local * group_size * head_dim).astype(jnp.bfloat16)


def on_device(
    queries,
    keys_values,
    sink_logits,
    doc_ids,
    residual,
    out_weight,
    ffn_gain,
    gate_weight,
    value_weight,
    conv_taps,
    down_weight,
):
    local_rows = queries.shape[0]
    offset = lax.axis_index("sp") * local_rows
    tp_count = lax.axis_size("tp")
    part_rows = local_rows // tp_count
    row_start = lax.axis_index("tp") * part_rows
    gate_whole, value_whole, down_whole = (
        lax.all_gather(gate_weight, "sp", axis=0, tiled=True),
        lax.all_gather(value_weight, "sp", axis=0, tiled=True),
        lax.all_gather(down_weight, "sp", axis=0, tiled=True),
    )
    attended = attend(queries, keys_values, sink_logits, doc_ids, offset)
    partial_value = jnp.dot(attended, out_weight, preferred_element_type=jnp.float32)
    projected = lax.psum(partial_value.astype(jnp.bfloat16), "tp").astype(jnp.float32)
    stream = (residual.astype(jnp.float32) + projected).astype(jnp.bfloat16)
    normed = normalize(stream, ffn_gain)
    stream_rows = lax.dynamic_slice_in_dim(stream, row_start, part_rows, 0)
    gate_pre = jnp.dot(normed, gate_whole, preferred_element_type=jnp.float32)
    value_pre = jnp.dot(normed, value_whole, preferred_element_type=jnp.float32)
    gate_stored = gate_pre.astype(jnp.bfloat16)
    extended = extended_2(gate_stored, (("sp", 0),), 1).astype(jnp.float32)
    padded_docs = jnp.pad(doc_ids, 1, constant_values=-1)
    near_docs = lax.dynamic_slice_in_dim(padded_docs, offset, local_rows + 2)
    prev_same = (near_docs[1:-1] == near_docs[:-2]).astype(jnp.float32)[:, None]
    next_same = (near_docs[1:-1] == near_docs[2:]).astype(jnp.float32)[:, None]
    conved = (
        conv_taps[0] * extended[:-2] * prev_same
        + conv_taps[1] * extended[1:-1]
        + conv_taps[2] * extended[2:] * next_same
    )
    hidden = (jax.nn.gelu(conved, approximate=True) * value_pre).astype(jnp.bfloat16)
    lowered = lax.psum_scatter(
        lax.dot_general(
            hidden, down_whole, contract_last, preferred_element_type=jnp.float32
        ).astype(jnp.bfloat16),
        "tp",
        scatter_dimension=0,
        tiled=True,
    ).astype(jnp.float32)
    return (stream_rows.astype(jnp.float32) + lowered).astype(jnp.bfloat16)


def solution(mesh):
    in_specs = (
        P("sp", "tp", None),
        P("sp", "tp", None),
        P("tp", None),
        P(),
        P("sp", None),
        P("tp", None),
        P(),
        P("sp", "tp"),
        P("sp", "tp"),
        P(None, "tp"),
        P("sp", "tp"),
    )
    out_specs = P(("sp", "tp"), None)
    return jax.shard_map(
        on_device, mesh=mesh, in_specs=in_specs, out_specs=out_specs, check_vma=False
    )
```

profile of v0, /device:TPU:0, one launch (start us, length us, event | category | flops | bytes accessed | tf_op | source)
XLA Modules:
  0.0 373.3 jit_solution(15646280819645604768)
XLA Ops:
  7.4 1.2 copy.14
  8.6 4.9 %collective-permute-start = (bf16[128,2,128]{2,0,1:T(8,128)(2,1)S(1)}, bf16[128,2,128]{2,0,1:T(8,128)(2,1)S(1)}, u32[]{:S(2)}, u32[]{:S(2)}) collective-permute-start(bf16[128,2,128]{2,0,1:T(8,128)(2,1)S(1)} %get-tuple-element.14), channel_id=1, source_target_pairs={{0,4},{4,8},{8,12},{12,16},{16,20},{20,24},{24,28},{1,5},{5,9},{9,... | collective-permute-start | bytes 196616 | tf_op jit(solution)/shard_map/ppermute | solution.py:21
  13.5 1.3 collective-permute-start.1
  14.9 0.9 fusion.31
  16.4 1.3 copy.20
  17.7 3.7 reshape.100
  22.0 1.0 pad_maximum_fusion.2
  23.9 2.5 fusion.17
  26.4 1.6 fusion.3
  28.1 1.8 fusion.20
  30.2 3.2 convolution_convert_fusion.2
  35.6 86.5 %all-reduce.4.cloned.1.call-done = bf16[1024,2048]{1,0:T(8,128)(2,1)} async-done(((bf16[1024,2048]{1,0:T(8,128)(2,1)}), bf16[1024,2048]{1,0:T(8,128)(2,1)}) %all-reduce.4.cloned.1.call-update) | async-done | bytes 4194320 | tf_op jit(solution)/shard_map/psum | solution.py:99
  122.1 7.4 %fusion = (f32[1024]{0:T(1024)S(1)}, bf16[1024,2048]{1,0:T(8,128)(2,1)}) fusion(bf16[1024,2048]{1,0:T(8,128)(2,1)} %all-reduce.4.cloned.1.call-done, bf16[1024,2048]{1,0:T(8,128)(2,1)} %param.15), kind=kLoop, calls=%fused_computation.2 | loop fusion | flops 14679040 | bytes 12587008 | tf_op jit(solution)/shard_map/reduce_sum | solution.py:37
  129.5 9.3 %convolution_convert_fusion = bf16[1024,1280]{1,0:T(8,128)(2,1)S(1)} fusion(bf16[2048,1280]{1,0:T(8,128)(2,1)} %all-gather.4.cloned.1.call-done, bf16[1024,2048]{1,0:T(8,128)(2,1)} %get-tuple-element.9, f32[2048]{0:T(1024)S(1)} %copy-done.7, f32[1024]{0:T(1024)S(1)} %add_rsqrt_fusion), kind=kOutput, calls=%fused_computation.28 | convolution fusion | flops 5378408448 | bytes 12070912 | tf_op jit(solution)/shard_map/dot_general | solution.py:103
  138.8 3.3 collective-permute-start.2
  142.2 1.3 collective-permute-start.3
  143.6 4.1 %collective-permute-done.3 = bf16[1,1280]{1,0:T(2,128)(2,1)S(1)} collective-permute-done((bf16[1,1280]{1,0:T(2,128)(2,1)S(1)}, bf16[1,1280]{1,0:T(2,128)(2,1)S(1)}, u32[]{:S(2)}, u32[]{:S(2)}) %collective-permute-start.3) | collective-permute-done | bytes 2592 | tf_op jit(solution)/shard_map/ppermute | solution.py:23
  147.7 13.4 %concatenate.20 = bf16[1026,1280]{1,0:T(8,128)(2,1)S(1)} concatenate(bf16[1,1280]{1,0:T(2,128)(2,1)S(1)} %collective-permute-done.2, bf16[1024,1280]{1,0:T(8,128)(2,1)} %copy-done.2, bf16[1,1280]{1,0:T(2,128)(2,1)S(1)} %collective-permute-done.3), dimensions={0} | concatenate | bytes 5253120 | tf_op jit(solution)/shard_map/concatenate | solution.py:19
  161.0 2.7 convert_element_type.69
  163.8 47.1 %all-gather.6.cloned.1.call-done = bf16[2048,1280]{1,0:T(8,128)(2,1)} async-done(((bf16[256,1280]{1,0:T(8,128)(2,1)}), bf16[2048,1280]{1,0:T(8,128)(2,1)}) %all-gather.6.cloned.1.call-update) | async-done | bytes 5242896 | tf_op jit(solution)/shard_map/all_gather | solution.py:94
  210.9 86.0 %all-gather.8.cloned.1.call-done = bf16[2048,1280]{1,0:T(8,128)(2,1)} async-done(((bf16[256,1280]{1,0:T(8,128)(2,1)}), bf16[2048,1280]{1,0:T(8,128)(2,1)}) %all-gather.8.cloned.1.call-update) | async-done | bytes 5242896 | tf_op jit(solution)/shard_map/all_gather | solution.py:95
  296.8 22.9 %convolution_convert_fusion.1 = bf16[1024,2048]{1,0:T(8,128)(2,1)} fusion(bf16[2048,1280]{1,0:T(8,128)(2,1)} %all-gather.8.cloned.1.call-done, f32[1026,1280]{1,0:T(8,128)} %convert_element_type.69, bf16[2048,1280]{1,0:T(8,128)(2,1)} %all-gather.6.cloned.1.call-done, f32[1024]{0:T(1024)S(1)} %get-tuple-element.17, f32[1280]{0:T(1024)S(1)} %get-tuple-element.6, ...), kind=kOutput, calls=%fused_computation.29 | convolution fusion | flops 10770186240 | bytes 34638848 | tf_op jit(solution)/shard_map/dot_general | solution.py:118
  319.8 43.0 %reduce-scatter.2.cloned.1.call-done = bf16[256,2048]{1,0:T(8,128)(2,1)} async-done(((bf16[1024,2048]{1,0:T(8,128)(2,1)}), bf16[256,2048]{1,0:T(8,128)(2,1)}) %reduce-scatter.2.cloned.1.call-update) | async-done | bytes 1048592 | tf_op jit(solution)/shard_map/reduce_scatter | solution.py:117
  362.8 2.9 add_convert_fusion.1
  (45 shorter events, 4.7 us)
Async XLA Ops:
  7.4 22.8 %copy-start = (bf16[256,2048]{1,0:T(8,128)(2,1)S(1)}, bf16[256,2048]{1,0:T(8,128)(2,1)}, u32[]{:S(2)}) copy-start(bf16[256,2048]{1,0:T(8,128)(2,1)} %param.16) | copy-start | bytes 3145732
  7.4 114.7 %all-reduce.4.cloned.1.call-start = ((), (), s32[]{:S(2)}) async-start(), calls=%async_computation.1 | async-start | bytes 8388608 | tf_op jit(solution)/shard_map/psum | solution.py:99
  8.6 12.8 %collective-permute-start = (bf16[128,2,128]{2,0,1:T(8,128)(2,1)S(1)}, bf16[128,2,128]{2,0,1:T(8,128)(2,1)S(1)}, u32[]{:S(2)}, u32[]{:S(2)}) collective-permute-start(bf16[128,2,128]{2,0,1:T(8,128)(2,1)S(1)} %get-tuple-element.14), channel_id=1, source_target_pairs={{0,4},{4,8},{8,12},{12,16},{16,20},{20,24},{24,28},{1,5},{5,9},{9,... | collective-permute-start | bytes 196616 | tf_op jit(solution)/shard_map/ppermute | solution.py:21
  13.5 8.5 %collective-permute-start.1 = (bf16[128,2,128]{2,0,1:T(8,128)(2,1)S(1)}, bf16[128,2,128]{2,0,1:T(8,128)(2,1)}, u32[]{:S(2)}, u32[]{:S(2)}) collective-permute-start(bf16[128,2,128]{2,0,1:T(8,128)(2,1)S(1)} %get-tuple-element.15), channel_id=1, source_target_pairs={{4,0},{8,4},{12,8},{16,12},{20,16},{24,20},{28,24},{5,1},{9,5},{13... | collective-permute-start | bytes 196616 | tf_op jit(solution)/shard_map/ppermute | solution.py:23
  21.4 0.6 copy-start.4
  23.6 2.8 copy-start.6
  30.2 5.3 %copy-start.5 = (f32[3,1280]{1,0:T(4,128)S(1)}, f32[3,1280]{1,0:T(4,128)}, u32[]{:S(2)}) copy-start(f32[3,1280]{1,0:T(4,128)} %param.20) | copy-start | bytes 46084
  33.5 96.0 %all-gather.4.cloned.1.call-start = ((), (), s32[]{:S(2)}) async-start(), calls=%async_computation.2 | async-start | bytes 5898240 | tf_op jit(solution)/shard_map/all_gather | solution.py:93
  34.1 176.8 %all-gather.6.cloned.1.call-start = ((), (), s32[]{:S(2)}) async-start(), calls=%async_computation.3 | async-start | bytes 5898240 | tf_op jit(solution)/shard_map/all_gather | solution.py:94
  34.7 262.2 %all-gather.8.cloned.1.call-start = ((), (), s32[]{:S(2)}) async-start(), calls=%async_computation.4 | async-start | bytes 5898240 | tf_op jit(solution)/shard_map/all_gather | solution.py:95
  35.3 327.5 %reduce-scatter.2.cloned.1.call-start = ((), (), s32[]{:S(2)}) async-start(), calls=%async_computation.5 | async-start | bytes 5242880 | tf_op jit(solution)/shard_map/reduce_scatter | solution.py:117
  35.5 93.9 %copy-start.7 = (f32[2048]{0:T(1024)S(1)}, f32[2048]{0:T(1024)}, u32[]{:S(2)}) copy-start(f32[2048]{0:T(1024)} %param.17) | copy-start | bytes 24580
  129.5 14.0 %copy-start.3 = (s32[8192]{0:T(1024)S(1)}, s32[8192]{0:T(1024)}, u32[]{:S(2)}) copy-start(s32[8192]{0:T(1024)} %param.14) | copy-start | bytes 98308
  138.8 4.8 %copy-start.2 = (bf16[1024,1280]{1,0:T(8,128)(2,1)}, bf16[1024,1280]{1,0:T(8,128)(2,1)S(1)}, u32[]{:S(2)}) copy-start(bf16[1024,1280]{1,0:T(8,128)(2,1)S(1)} %convolution_convert_fusion) | copy-start | bytes 7864324
  138.8 4.7 %collective-permute-start.2 = (bf16[1,1280]{1,0:T(2,128)(2,1)S(1)}, bf16[1,1280]{1,0:T(2,128)(2,1)S(1)}, u32[]{:S(2)}, u32[]{:S(2)}) collective-permute-start(bf16[1,1280]{1,0:T(2,128)(2,1)S(1)} %get-tuple-element.11), channel_id=1, source_target_pairs={{0,4},{4,8},{8,12},{12,16},{16,20},{20,24},{24,28},{1,5},{5,9},{9,... | collective-permute-start | bytes 7688 | tf_op jit(solution)/shard_map/ppermute | solution.py:21
  142.2 5.5 %collective-permute-start.3 = (bf16[1,1280]{1,0:T(2,128)(2,1)S(1)}, bf16[1,1280]{1,0:T(2,128)(2,1)S(1)}, u32[]{:S(2)}, u32[]{:S(2)}) collective-permute-start(bf16[1,1280]{1,0:T(2,128)(2,1)S(1)} %get-tuple-element.10), channel_id=1, source_target_pairs={{4,0},{8,4},{12,8},{16,12},{20,16},{24,20},{28,24},{5,1},{9,5},{13... | collective-permute-start | bytes 7688 | tf_op jit(solution)/shard_map/ppermute | solution.py:23
  296.8 68.8 %copy-start.1 = (bf16[256,2048]{1,0:T(8,128)(2,1)S(1)}, bf16[256,2048]{1,0:T(8,128)(2,1)}, u32[]{:S(2)}) copy-start(bf16[256,2048]{1,0:T(8,128)(2,1)} %param.16) | copy-start | bytes 3145732
Sparse Core Ops, SparseCore 0:
  33.6 88.4 all-reduce.3
  319.9 42.8 reduce-scatter.1
Sparse Core Ops, SparseCore 1:
  36.2 88.5 all-gather.3
  126.8 84.0 all-gather.5
  212.9 83.9 all-gather.7
where the time goes:
time: 374 us; the launch traced here: 373 us
  waiting for transfers between devices  268 us (72%)
  matrix products  39.7 us (11%)
  local copies, waits for them, and re-layouts  22.1 us (6%)
  other arithmetic  16.8 us (4%)
  between operations  15.3 us (4%)
  starting transfers between devices  11.1 us (3%)
    psum x1, waiting for transfers between devices, on_device(): lax.psum(partial_value.astype(jnp.bfloat16), 'tp').astype(jnp.float32)  86.5 us
    all_gather x1, waiting for transfers between devices, on_device(): lax.all_gather(down_weight, 'sp', axis=0, tiled=True)  86 us
    all_gather x1, waiting for transfers between devices, on_device(): lax.all_gather(value_weight, 'sp', axis=0, tiled=True)  47.1 us
    reduce_scatter x1, waiting for transfers between devices, on_device(): lax.psum_scatter(lax.dot_general(hidden, down_whole, contract_last, prefe...  43 us
    dot_general x1, matrix products, on_device(): lax.dot_general(hidden, down_whole, contract_last, preferred_element_type...  22.9 us
    concatenate x1, local copies, waits for them, and re-layouts, extended_2(): jnp.concatenate([lax.ppermute(tail, axis, [(i, (i + 1) % count) for i in...  13.4 us
    dot_general x1, matrix products, on_device(): gate_pre = jnp.dot(normed, gate_whole, preferred_element_type=jnp.float32)  9.3 us
    ppermute x2, starting transfers between devices, extended_2(): lax.ppermute(tail, axis, [(i, (i + 1) % count) for i in range(ends)])  8.22 us
  transfers between devices with their start and end apart: 9, of which 5 were waited for; matrix products, arithmetic and copies ran while one was open for 11% of the time, Pallas kernels for 0%

commit v1 on v0

--- a/solution.py
+++ b/solution.py
@@ -8,6 +8,16 @@
 norm_epsilon = 1e-06
 masked_score = -1e30
 contract_last = (((1,), (1,)), ((), ()))
+
+
+def stocks_see(piece_in, mesh_ax, dim_no=0):
+    frame_out = jnp.concatenate(
+        lax.all_to_all(
+            jnp.stack(tuple((piece_in for _ in range(lax.axis_size(mesh_ax))))), mesh_ax, 0, 0
+        ),
+        dim_no,
+    )
+    return frame_out
 
 
 def extended_2(cells, sides, width):
@@ -91,7 +101,7 @@
     row_start = lax.axis_index("tp") * part_rows
     gate_whole, value_whole, down_whole = (
         lax.all_gather(gate_weight, "sp", axis=0, tiled=True),
-        lax.all_gather(value_weight, "sp", axis=0, tiled=True),
+        stocks_see(value_weight, "sp"),
         lax.all_gather(down_weight, "sp", axis=0, tiled=True),
     )
     attended = attend(queries, keys_values, sink_logits, doc_ids, offset)

time: 374 us -> 380 us (1.016)
  waiting for transfers between devices: 268 us -> 258 us
  starting transfers between devices: 11.1 us -> 18.7 us
  local copies, waits for them, and re-layouts: 22.1 us -> 29.5 us
    all_gather x1, waiting for transfers between devices: 0.01 us -> 87.7 us  [on_device(): lax.all_gather(gate_weight, 'sp', axis=0, tiled=True)]
    all_gather x1 -> x0, waiting for transfers between devices: 47.1 us -> none  [on_device(): lax.all_gather(value_weight, 'sp', axis=0, tiled=True)]
    all_gather x1, waiting for transfers between devices: 86 us -> 45.2 us  [on_device(): lax.all_gather(down_weight, 'sp', axis=0, tiled=True)]
    psum x1, waiting for transfers between devices: 86.5 us -> 76.8 us  [on_device(): lax.psum(partial_value.astype(jnp.bfloat16), 'tp').astype(jnp.float32)]
    all_to_all x0 -> x1, starting transfers between devices: none -> 7.66 us  [stocks_see(): lax.all_to_all(jnp.stack(tuple((piece_in for _ in range(lax.axis_size(mes...]
  transfers between devices with their start and end apart: 9 -> 9, of which waited for: 5 -> 5; matrix products, arithmetic and copies ran while one was open for 11% -> 12% of each run, Pallas kernels for 0% -> 0%
where the time goes in v1:
time: 380 us; the launch traced here: 379 us
  waiting for transfers between devices  258 us (68%)
  matrix products  39.5 us (10%)
  local copies, waits for them, and re-layouts  29.5 us (8%)
  starting transfers between devices  18.7 us (5%)
  other arithmetic  18.4 us (5%)
  between operations  15.1 us (4%)
    all_gather x1, waiting for transfers between devices, on_device(): lax.all_gather(gate_weight, 'sp', axis=0, tiled=True)  87.7 us
    psum x1, waiting for transfers between devices, on_device(): lax.psum(partial_value.astype(jnp.bfloat16), 'tp').astype(jnp.float32)  76.8 us
    all_gather x1, waiting for transfers between devices, on_device(): lax.all_gather(down_weight, 'sp', axis=0, tiled=True)  45.2 us
    reduce_scatter x1, waiting for transfers between devices, on_device(): lax.psum_scatter(lax.dot_general(hidden, down_whole, contract_last, prefe...  43 us
    dot_general x1, matrix products, on_device(): lax.dot_general(hidden, down_whole, contract_last, preferred_element_type...  22.8 us
    concatenate x1, local copies, waits for them, and re-layouts, extended_2(): jnp.concatenate([lax.ppermute(tail, axis, [(i, (i + 1) % count) for i in...  16.7 us
    dot_general x1, matrix products, on_device(): gate_pre = jnp.dot(normed, gate_whole, preferred_element_type=jnp.float32)  9.2 us
    ppermute x2, starting transfers between devices, extended_2(): lax.ppermute(tail, axis, [(i, (i + 1) % count) for i in range(ends)])  8.12 us
  transfers between devices with their start and end apart: 9, of which 5 were waited for; matrix products, arithmetic and copies ran while one was open for 12% of the time, Pallas kernels for 0%

profile of v1, /device:TPU:0, one launch (start us, length us, event | category | flops | bytes accessed | tf_op | source)
XLA Modules:
  0.0 379.1 jit_solution(8039133650471578305)
XLA Ops:
  8.6 4.9 %collective-permute-start = (bf16[128,2,128]{2,0,1:T(8,128)(2,1)S(1)}, bf16[128,2,128]{2,0,1:T(8,128)(2,1)S(1)}, u32[]{:S(2)}, u32[]{:S(2)}) collective-permute-start(bf16[128,2,128]{2,0,1:T(8,128)(2,1)S(1)} %get-tuple-element.14), channel_id=1, source_target_pairs={{0,4},{4,8},{8,12},{12,16},{16,20},{20,24},{24,28},{1,5},{5,9},{9,... | collective-permute-start | bytes 196616 | tf_op jit(solution)/shard_map/ppermute | solution.py:31
  13.5 1.3 collective-permute-start.1
  16.4 1.3 copy.20
  17.7 3.7 reshape.106
  23.9 2.5 fusion.17
  26.4 1.5 fusion.3
  28.0 1.8 fusion.20
  30.2 3.3 convolution_convert_fusion.2
  34.0 2.6 stack.2
  36.6 7.7 %all-to-all-start = ((bf16[8,256,1280]{2,1,0:T(8,128)(2,1)}), bf16[8,256,1280]{2,1,0:T(8,128)(2,1)}, u32[]{:S(2)}, u32[]{:S(2)}) async-start(bf16[8,256,1280]{2,1,0:T(8,128)(2,1)} %stack.2), calls=%async_computation | async-start | bytes 10485760 | tf_op jit(solution)/shard_map/all_to_all | solution.py:15
  45.2 76.8 %all-reduce.4.cloned.1.call-done = bf16[1024,2048]{1,0:T(8,128)(2,1)} async-done(((bf16[1024,2048]{1,0:T(8,128)(2,1)}), bf16[1024,2048]{1,0:T(8,128)(2,1)}) %all-reduce.4.cloned.1.call-update) | async-done | bytes 4194320 | tf_op jit(solution)/shard_map/psum | solution.py:109
  122.0 7.4 %fusion = (f32[1024]{0:T(1024)S(1)}, bf16[1024,2048]{1,0:T(8,128)(2,1)}) fusion(bf16[1024,2048]{1,0:T(8,128)(2,1)} %all-reduce.4.cloned.1.call-done, bf16[1024,2048]{1,0:T(8,128)(2,1)} %param.15), kind=kLoop, calls=%fused_computation.2 | loop fusion | flops 14679040 | bytes 12587008 | tf_op jit(solution)/shard_map/reduce_sum | solution.py:47
  129.4 87.7 %all-gather.3.cloned.1.call-done = bf16[2048,1280]{1,0:T(8,128)(2,1)} async-done(((bf16[256,1280]{1,0:T(8,128)(2,1)}), bf16[2048,1280]{1,0:T(8,128)(2,1)}) %all-gather.3.cloned.1.call-update) | async-done | bytes 5242896 | tf_op jit(solution)/shard_map/all_gather | solution.py:103
  217.1 9.2 %convolution_convert_fusion = bf16[1024,1280]{1,0:T(8,128)(2,1)S(1)} fusion(bf16[2048,1280]{1,0:T(8,128)(2,1)} %all-gather.3.cloned.1.call-done, bf16[1024,2048]{1,0:T(8,128)(2,1)} %get-tuple-element.9, f32[2048]{0:T(1024)S(1)} %copy-done.8, f32[1024]{0:T(1024)S(1)} %add_rsqrt_fusion), kind=kOutput, calls=%fused_computation.28 | convolution fusion | flops 5378408448 | bytes 12070912 | tf_op jit(solution)/shard_map/dot_general | solution.py:113
  226.4 1.5 copy-done.2
  227.9 3.2 collective-permute-start.2
  231.1 1.3 collective-permute-start.3
  232.5 4.1 %collective-permute-done.3 = bf16[1,1280]{1,0:T(2,128)(2,1)S(1)} collective-permute-done((bf16[1,1280]{1,0:T(2,128)(2,1)S(1)}, bf16[1,1280]{1,0:T(2,128)(2,1)S(1)}, u32[]{:S(2)}, u32[]{:S(2)}) %collective-permute-start.3) | collective-permute-done | bytes 2592 | tf_op jit(solution)/shard_map/ppermute | solution.py:33
  236.6 16.7 %concatenate.20 = bf16[1026,1280]{1,0:T(8,128)(2,1)} concatenate(bf16[1,1280]{1,0:T(2,128)(2,1)S(1)} %collective-permute-done.2, bf16[1024,1280]{1,0:T(8,128)(2,1)} %copy-done.2, bf16[1,1280]{1,0:T(2,128)(2,1)S(1)} %collective-permute-done.3), dimensions={0} | concatenate | bytes 5253120 | tf_op jit(solution)/shard_map/concatenate | solution.py:29
  253.3 4.4 %convert_element_type.69 = f32[1026,1280]{1,0:T(8,128)} convert(bf16[1026,1280]{1,0:T(8,128)(2,1)} %concatenate.20) | non-fusion elementwise | flops 1313280 | bytes 7879680 | tf_op jit(solution)/shard_map/convert_element_type | solution.py:116
  257.7 45.2 %all-gather.5.cloned.1.call-done = bf16[2048,1280]{1,0:T(8,128)(2,1)} async-done(((bf16[256,1280]{1,0:T(8,128)(2,1)}), bf16[2048,1280]{1,0:T(8,128)(2,1)}) %all-gather.5.cloned.1.call-update) | async-done | bytes 5242896 | tf_op jit(solution)/shard_map/all_gather | solution.py:105
  303.0 22.8 %convolution_convert_fusion.1 = bf16[1024,2048]{1,0:T(8,128)(2,1)} fusion(bf16[2048,1280]{1,0:T(8,128)(2,1)} %all-gather.5.cloned.1.call-done, f32[1026,1280]{1,0:T(8,128)} %convert_element_type.69, bf16[2048,1280]{1,0:T(8,128)(2,1)} %bitcast.12, f32[1024]{0:T(1024)S(1)} %get-tuple-element.17, f32[1280]{0:T(1024)S(1)} %get-tuple-element.6, ...), kind=kOutput, calls=%fused_computation.29 | convolution fusion | flops 10770186240 | bytes 34638848 | tf_op jit(solution)/shard_map/dot_general | solution.py:128
  325.8 43.0 %reduce-scatter.2.cloned.1.call-done = bf16[256,2048]{1,0:T(8,128)(2,1)} async-done(((bf16[1024,2048]{1,0:T(8,128)(2,1)}), bf16[256,2048]{1,0:T(8,128)(2,1)}) %reduce-scatter.2.cloned.1.call-update) | async-done | bytes 1048592 | tf_op jit(solution)/shard_map/reduce_scatter | solution.py:127
  368.8 2.9 add_convert_fusion.1
  (47 shorter events, 7.3 us)
Async XLA Ops:
  7.4 22.8 %copy-start = (bf16[256,2048]{1,0:T(8,128)(2,1)S(1)}, bf16[256,2048]{1,0:T(8,128)(2,1)}, u32[]{:S(2)}) copy-start(bf16[256,2048]{1,0:T(8,128)(2,1)} %param.16) | copy-start | bytes 3145732
  7.4 114.7 %all-reduce.4.cloned.1.call-start = ((), (), s32[]{:S(2)}) async-start(), calls=%async_computation.2 | async-start | bytes 8388608 | tf_op jit(solution)/shard_map/psum | solution.py:109
  8.6 12.8 %collective-permute-start = (bf16[128,2,128]{2,0,1:T(8,128)(2,1)S(1)}, bf16[128,2,128]{2,0,1:T(8,128)(2,1)S(1)}, u32[]{:S(2)}, u32[]{:S(2)}) collective-permute-start(bf16[128,2,128]{2,0,1:T(8,128)(2,1)S(1)} %get-tuple-element.14), channel_id=1, source_target_pairs={{0,4},{4,8},{8,12},{12,16},{16,20},{20,24},{24,28},{1,5},{5,9},{9,... | collective-permute-start | bytes 196616 | tf_op jit(solution)/shard_map/ppermute | solution.py:31
  13.5 8.5 %collective-permute-start.1 = (bf16[128,2,128]{2,0,1:T(8,128)(2,1)S(1)}, bf16[128,2,128]{2,0,1:T(8,128)(2,1)}, u32[]{:S(2)}, u32[]{:S(2)}) collective-permute-start(bf16[128,2,128]{2,0,1:T(8,128)(2,1)S(1)} %get-tuple-element.15), channel_id=1, source_target_pairs={{4,0},{8,4},{12,8},{16,12},{20,16},{24,20},{28,24},{5,1},{9,5},{13... | collective-permute-start | bytes 196616 | tf_op jit(solution)/shard_map/ppermute | solution.py:33
  21.4 0.6 copy-start.5
  23.6 2.8 copy-start.7
  30.2 3.9 %copy-start.3 = (bf16[256,1280]{1,0:T(8,128)(2,1)S(1)}, bf16[256,1280]{1,0:T(8,128)(2,1)}, u32[]{:S(2)}) copy-start(bf16[256,1280]{1,0:T(8,128)(2,1)} %param.19) | copy-start | bytes 1966084
  33.5 183.7 %all-gather.3.cloned.1.call-start = ((), (), s32[]{:S(2)}) async-start(), calls=%async_computation.3 | async-start | bytes 5898240 | tf_op jit(solution)/shard_map/all_gather | solution.py:103
  36.6 8.5 %copy-start.6 = (f32[3,1280]{1,0:T(4,128)S(1)}, f32[3,1280]{1,0:T(4,128)}, u32[]{:S(2)}) copy-start(f32[3,1280]{1,0:T(4,128)} %param.20) | copy-start | bytes 46084
  36.6 221.1 %all-to-all-start = ((bf16[8,256,1280]{2,1,0:T(8,128)(2,1)}), bf16[8,256,1280]{2,1,0:T(8,128)(2,1)}, u32[]{:S(2)}, u32[]{:S(2)}) async-start(bf16[8,256,1280]{2,1,0:T(8,128)(2,1)} %stack.2), calls=%async_computation | async-start | bytes 10485760 | tf_op jit(solution)/shard_map/all_to_all | solution.py:15
  44.3 258.7 %all-gather.5.cloned.1.call-start = ((), (), s32[]{:S(2)}) async-start(), calls=%async_computation.4 | async-start | bytes 5898240 | tf_op jit(solution)/shard_map/all_gather | solution.py:105
  44.9 323.9 %reduce-scatter.2.cloned.1.call-start = ((), (), s32[]{:S(2)}) async-start(), calls=%async_computation.5 | async-start | bytes 5242880 | tf_op jit(solution)/shard_map/reduce_scatter | solution.py:127
  45.2 172.0 %copy-start.8 = (f32[2048]{0:T(1024)S(1)}, f32[2048]{0:T(1024)}, u32[]{:S(2)}) copy-start(f32[2048]{0:T(1024)} %param.17) | copy-start | bytes 24580
  217.1 15.3 %copy-start.4 = (s32[8192]{0:T(1024)S(1)}, s32[8192]{0:T(1024)}, u32[]{:S(2)}) copy-start(s32[8192]{0:T(1024)} %param.14) | copy-start | bytes 98308
  226.3 1.5 copy-start.2
  227.9 4.6 %collective-permute-start.2 = (bf16[1,1280]{1,0:T(2,128)(2,1)S(1)}, bf16[1,1280]{1,0:T(2,128)(2,1)S(1)}, u32[]{:S(2)}, u32[]{:S(2)}) collective-permute-start(bf16[1,1280]{1,0:T(2,128)(2,1)S(1)} %get-tuple-element.11), channel_id=1, source_target_pairs={{0,4},{4,8},{8,12},{12,16},{16,20},{20,24},{24,28},{1,5},{5,9},{9,... | collective-permute-start | bytes 7688 | tf_op jit(solution)/shard_map/ppermute | solution.py:31
  231.1 5.5 %collective-permute-start.3 = (bf16[1,1280]{1,0:T(2,128)(2,1)S(1)}, bf16[1,1280]{1,0:T(2,128)(2,1)S(1)}, u32[]{:S(2)}, u32[]{:S(2)}) collective-permute-start(bf16[1,1280]{1,0:T(2,128)(2,1)S(1)} %get-tuple-element.10), channel_id=1, source_target_pairs={{4,0},{8,4},{12,8},{16,12},{20,16},{24,20},{28,24},{5,1},{9,5},{13... | collective-permute-start | bytes 7688 | tf_op jit(solution)/shard_map/ppermute | solution.py:33
  303.0 68.7 %copy-start.1 = (bf16[256,2048]{1,0:T(8,128)(2,1)S(1)}, bf16[256,2048]{1,0:T(8,128)(2,1)}, u32[]{:S(2)}) copy-start(bf16[256,2048]{1,0:T(8,128)(2,1)} %param.16) | copy-start | bytes 3145732
Sparse Core Ops, SparseCore 0:
  33.6 88.3 all-reduce.3
  326.0 42.7 reduce-scatter.1
Sparse Core Ops, SparseCore 1:
  36.1 180.9 all-gather.2
  219.2 83.7 all-gather.4
